TPU v7x, 128 devices: a whole 4x4x4 slice. The times are simulated.
128 devices in a mesh: kv: 16 (over z, y), tp: 8 (over x, core).
Axes of the slice: x: 4, y: 4, z: 4, core: 2. Of those that a mesh axis runs over, the one named last changes fastest.
Arguments:
- tokens: bfloat16 [2048, 4096], P(None, 'kv'), may hold values from -6 to 6
- norm_gain: float32 [4096], replicated, may hold values from 0.1 to 1.9
- query_weight: bfloat16 [4096, 2048], P('kv', 'tp'), may hold values from -0.09375 to 0.09375
- key_weight: bfloat16 [4096, 2048], P('kv', 'tp'), may hold values from -0.09375 to 0.09375
- value_weight: bfloat16 [4096, 4096], P('kv', 'tp'), may hold values from -0.09375 to 0.09375
- outgate_weight: bfloat16 [4096, 4096], P('kv', 'tp'), may hold values from -0.09375 to 0.09375
- gate_weight: bfloat16 [4096, 32], P('kv'), may hold values from -0.09375 to 0.09375
- forget_bias: float32 [16], replicated, may hold values from -1 to 5
- head_gain: float32 [4096], P('tp'), may hold values from 0.1 to 1.9
- output_weight: bfloat16 [4096, 4096], P('tp', 'kv'), may hold values from -0.09375 to 0.09375
- state_matrix: float32 [512, 16, 128, 256], P('kv', 'tp'), may hold values from -6 to 6
- state_normal: float32 [512, 16, 128], P('kv', 'tp'), may hold values from -6 to 6
- state_stable: float32 [512, 16], P('kv', 'tp'), may hold values from -3 to 3
- prior_keys: bfloat16 [512, 4, 2048], P('kv', None, 'tp'), may hold values from -0.59765625 to 0.59765625
- prior_values: bfloat16 [512, 4, 4096], P('kv', None, 'tp'), may hold values from -6 to 6
- prior_ingate: float32 [512, 4, 16], P('kv', None, 'tp'), may hold values from -4 to 4
- prior_forget: float32 [512, 4, 16], P('kv', None, 'tp'), may hold values from -2 to -0.02
- accepted: int32 [512], P('kv'), may hold values from 0 to 4
- parents: int32 [512, 4], P('kv'), may hold values from -1 to 2, as said below
Outputs:
- layer_out: bfloat16 [2048, 4096], P('tp', 'kv')
- new_matrix: float32 [512, 16, 128, 256], P('kv', 'tp')
- new_normal: float32 [512, 16, 128], P('kv', 'tp')
- new_stable: float32 [512, 16], P('kv', 'tp')
Inputs may be any that keep to these rules, and one draw needn't show every extreme that they name: parents of proposal t lie in -1 to t - 1; the first proposal's parent is -1; in some sequence each proposal's parent is the one before it.
All inputs are finite; a program needn't handle non-finite values.
Results may differ from a plain program's by a relative error of at most 0.0089.
Values may be sent and summed in bfloat16 or wider, within the bound.
A program may use at most 128 MiB of HBM per device.

v0:
```python
import jax
import jax.numpy as jnp
from jax import lax
from jax.sharding import Mesh
from jax.sharding import PartitionSpec as P

D = 4096
HEADS = 16
DQK = 128
DV = 256
PROP = 4
KV = ("kv_0", "kv_1")


def over_axes(value, axes):
    for axis in axes:
        value = lax.psum(value, axis)
    return value


def sent_together(arrays, axis, dim, along):
    widths = [a.shape[along] for a in arrays]
    both = jnp.concatenate(arrays, axis=along)
    filled = lax.psum_scatter(both, axis, scatter_dimension=dim, tiled=True)
    return tuple(jnp.split(filled, [sum(widths[:k]) for k in range(1, len(widths))], axis=along))


def from_everyone(value, axis):
    copies = jnp.broadcast_to(value, (lax.axis_size(axis), *value.shape))
    return lax.all_to_all(copies, axis, split_axis=0, concat_axis=0, tiled=True)


def laid_out(blocks, dim):
    blocks = jnp.moveaxis(blocks, 0, dim)
    lengths = blocks.shape
    return blocks.reshape(*lengths[:dim], lengths[dim] * lengths[dim + 1], *lengths[dim + 2 :])


def collect(value, axis, dim):
    blocks = from_everyone(value, axis)
    return laid_out(blocks, dim)


def split_up(value, dim, peers):
    lengths = value.shape
    blocks = value.reshape(*lengths[:dim], peers, lengths[dim] // peers, *lengths[dim + 1 :])
    return jnp.moveaxis(blocks, dim, 0)


def sum_at_owner(value, axis, dim):
    blocks = split_up(value, dim, lax.axis_size(axis))
    arrived = lax.all_to_all(blocks, axis, split_axis=0, concat_axis=0, tiled=True)
    return arrived.astype(jnp.float32).sum(axis=0)


def ancestry(parents):
    count = parents.shape[1]
    index = jnp.arange(count, dtype=jnp.int32)
    current = jnp.broadcast_to(index[None, :], parents.shape)
    table = jnp.broadcast_to(
        (index[:, None] == index[None, :]).astype(jnp.float32), (parents.shape[0], count, count)
    )
    for repeat in range(count - 1):
        looked = jnp.take_along_axis(parents, jnp.maximum(current, 0), axis=1)
        current = jnp.where(current >= 0, looked, -1)
        table = table + (current[:, :, None] == index[None, None, :]).astype(jnp.float32)
    return table


def commit(matrix, normal, stable, prior_k, prior_v, prior_i, prior_f, accepted):
    count = prior_k.shape[1]
    live = (jnp.arange(count, dtype=jnp.int32)[None, :] < accepted[:, None])[:, :, None]
    forget_live = jnp.where(live, prior_f, 0.0)
    cumul = jnp.cumsum(forget_live, axis=1)
    total = cumul[:, -1]
    weight_log = jnp.where(live, total[:, None, :] - cumul + prior_i, -jnp.inf)
    new_stable = jnp.maximum(total + stable, jnp.max(weight_log, axis=1))
    weights = jnp.exp(weight_log - new_stable[:, None, :])
    decay = jnp.exp(total + stable - new_stable)
    hp = lax.Precision.HIGHEST
    new_matrix = decay[:, :, None, None] * matrix + jnp.einsum(
        "sph,sphd,sphv->shdv", weights, prior_k, prior_v, precision=hp
    )
    new_normal = decay[:, :, None] * normal + jnp.einsum(
        "sph,sphd->shd", weights, prior_k, precision=hp
    )
    return (new_matrix, new_normal, new_stable)


def tree_read(query, key_rows, value_rows, ingate, logforget, table, matrix, normal, stable):
    hp = lax.Precision.HIGHEST
    path_sum = jnp.einsum("sta,sah->sth", table, logforget, precision=hp)
    dlog = path_sum[:, :, None, :] - path_sum[:, None, :, :] + ingate[:, None, :, :]
    dlog = jnp.where(table[:, :, :, None] > 0.5, dlog, -jnp.inf)
    carried = path_sum + stable[:, None, :]
    top = jnp.maximum(carried, jnp.max(dlog, axis=2))
    scores = jnp.einsum("sthd,sahd->stah", query, key_rows, precision=hp) * jnp.exp(
        dlog - top[:, :, None, :]
    )
    factor = jnp.exp(carried - top)
    numer = jnp.einsum("stah,sahv->sthv", scores, value_rows, precision=hp) + factor[
        ..., None
    ] * jnp.einsum("sthd,shdv->sthv", query, matrix, precision=hp)
    denom = jnp.sum(scores, axis=2) + factor * jnp.einsum(
        "sthd,shd->sth", query, normal, precision=hp
    )
    return numer / jnp.maximum(jnp.abs(denom), jnp.exp(-top))[..., None]


def head_gate_columns(gate_block, head_start, head_local):
    rows = gate_block.shape[0]
    picked = lax.dynamic_slice_in_dim(gate_block.reshape(rows, 2, HEADS), head_start, head_local, 2)
    return picked.reshape(rows, 2 * head_local)


def per_device(
    tokens,
    norm_gain,
    query_weight,
    key_weight,
    value_weight,
    outgate_weight,
    gate_weight,
    forget_bias,
    head_gain,
    output_weight,
    state_matrix,
    state_normal,
    state_stable,
    prior_keys,
    prior_values,
    prior_ingate,
    prior_forget,
    accepted,
    parents,
):
    f32 = jnp.float32
    head_local = query_weight.shape[1] // DQK
    width_local = tokens.shape[1]
    seq_local = accepted.shape[0]
    row_local = seq_local * PROP
    head_start = lax.axis_index("tp") * head_local
    xfloat = tokens.astype(f32)
    part_squares = jnp.sum(xfloat * xfloat, axis=-1)
    own_gain = lax.dynamic_slice_in_dim(norm_gain, lax.axis_index(KV) * width_local, width_local, 0)
    normed = (xfloat * own_gain).astype(jnp.bfloat16)
    gate_cols = head_gate_columns(gate_weight, head_start, head_local)
    part_query = jnp.dot(normed, query_weight, preferred_element_type=f32)
    part_key = jnp.dot(normed, key_weight, preferred_element_type=f32)
    part_value = jnp.dot(normed, value_weight, preferred_element_type=f32)
    part_outgate = jnp.dot(normed, outgate_weight, preferred_element_type=f32)
    part_gates = jnp.dot(normed, gate_cols, preferred_element_type=f32)
    all_squares = over_axes(part_squares, KV)
    query, key_rows, value_rows, outgate, gates = sent_together(
        (part_query, part_key, part_value, part_outgate, part_gates), KV, 0, 1
    )
    squares = lax.dynamic_slice_in_dim(all_squares, lax.axis_index(KV) * row_local, row_local, 0)
    scale = lax.rsqrt(squares / D + 1e-06)[:, None]
    query = (scale * query).reshape(seq_local, PROP, head_local, DQK)
    key_rows = (scale * key_rows / jnp.sqrt(jnp.float32(DQK))).reshape(
        seq_local, PROP, head_local, DQK
    )
    value_rows = (scale * value_rows).reshape(seq_local, PROP, head_local, DV)
    outgate = (scale * outgate).reshape(seq_local, PROP, head_local, DV)
    gates = scale * gates
    own_bias = lax.dynamic_slice_in_dim(forget_bias, head_start, head_local, 0)
    ingate = gates[:, :head_local].reshape(seq_local, PROP, head_local)
    logforget = jax.nn.log_sigmoid(gates[:, head_local:] + own_bias).reshape(
        seq_local, PROP, head_local
    )
    new_matrix, new_normal, new_stable = commit(
        state_matrix,
        state_normal,
        state_stable,
        prior_keys.astype(f32).reshape(seq_local, PROP, head_local, DQK),
        prior_values.astype(f32).reshape(seq_local, PROP, head_local, DV),
        prior_ingate,
        prior_forget,
        accepted,
    )
    table = ancestry(parents)
    read = tree_read(
        query, key_rows, value_rows, ingate, logforget, table, new_matrix, new_normal, new_stable
    )
    normer = lax.rsqrt(jnp.mean(read * read, axis=-1, keepdims=True) + 1e-06)
    hidden = read * normer * head_gain.reshape(head_local, DV) * jax.nn.sigmoid(outgate)
    hidden = hidden.reshape(row_local, head_local * DV).astype(jnp.bfloat16)
    partial_out = jnp.dot(collect(hidden, KV, 0), output_weight, preferred_element_type=f32)
    layer_out = sum_at_owner(partial_out.astype(jnp.bfloat16), "tp", 0).astype(jnp.bfloat16)
    return (layer_out, new_matrix, new_normal, new_stable)


def solution(mesh):
    torus = Mesh(mesh.devices.reshape(4, 4, mesh.shape["tp"]), ("kv_0", "kv_1", "tp"))
    placed = (
        P(None, KV),
        P(),
        P(KV, "tp"),
        P(KV, "tp"),
        P(KV, "tp"),
        P(KV, "tp"),
        P(KV, None),
        P(),
        P("tp"),
        P("tp", KV),
        P(KV, "tp", None, None),
        P(KV, "tp", None),
        P(KV, "tp"),
        P(KV, None, "tp"),
        P(KV, None, "tp"),
        P(KV, None, "tp"),
        P(KV, None, "tp"),
        P(KV),
        P(KV, None),
    )
    return jax.shard_map(
        per_device,
        mesh=torus,
        in_specs=placed,
        out_specs=(P("tp", KV), P(KV, "tp", None, None), P(KV, "tp", None), P(KV, "tp")),
        check_vma=False,
    )
```

profile of v0, /device:TPU:1, one launch (start us, length us, event | category | flops | bytes accessed | tf_op | source)
XLA Modules:
  0.0 213.7 jit_solution(13729913416724993071)
XLA Ops:
  7.2 0.8 constant_dynamic-slice_fusion
  8.1 0.8 dynamic_slice.13
  8.8 3.1 %convolution_dynamic-update-slice_fusion.3 = f32[2048,1540]{0,1:T(8,128)} fusion(bf16[256,256]{1,0:T(8,128)(2,1)} %param.23, bf16[2048,256]{1,0:T(8,128)(2,1)} %param.21, f32[256]{0:T(256)S(1)} %dynamic_slice.13), kind=kOutput, calls=%fused_computation.7 | convolution fusion | flops 270008320 | bytes 3277824 | tf_op jit(solution)/shard_map/dot_general | solution.py:148
  11.9 3.1 %convolution_dynamic-update-slice_fusion.2 = f32[2048,1540]{0,1:T(8,128)} fusion(f32[2048,1540]{0,1:T(8,128)} %convolution_dynamic-update-slice_fusion.3, bf16[256,256]{1,0:T(8,128)(2,1)} %param.24, bf16[2048,256]{1,0:T(8,128)(2,1)} %param.21, f32[256]{0:T(256)S(1)} %dynamic_slice.13), kind=kOutput, calls=%fused_computation.6 | convolution fusion | flops 270008320 | bytes 3277824 | tf_op jit(solution)/shard_map/dot_general | solution.py:149
  15.0 2.7 %convolution_dynamic-update-slice_fusion.1 = f32[2048,1540]{0,1:T(8,128)} fusion(f32[2048,1540]{0,1:T(8,128)} %convolution_dynamic-update-slice_fusion.2, bf16[256,512]{1,0:T(8,128)(2,1)S(1)} %copy-done, bf16[2048,256]{1,0:T(8,128)(2,1)S(1)} %copy-done.3, f32[256]{0:T(256)S(1)} %dynamic_slice.13), kind=kOutput, calls=%fused_computation.5 | convolution fusion | flops 538443776 | bytes 5506048 | tf_op jit(solution)/shard_map/dot_general | solution.py:150
  17.7 2.7 %convolution_dynamic-update-slice_fusion = f32[2048,1540]{0,1:T(8,128)} fusion(f32[2048,1540]{0,1:T(8,128)} %convolution_dynamic-update-slice_fusion.1, bf16[256,512]{1,0:T(8,128)(2,1)S(1)} %copy-done.4, bf16[2048,256]{1,0:T(8,128)(2,1)S(1)} %copy-done.3, f32[256]{0:T(256)S(1)} %dynamic_slice.13), kind=kOutput, calls=%fused_computation.4 | convolution fusion | flops 538443776 | bytes 5506048 | tf_op jit(solution)/shard_map/dot_general | solution.py:151
  20.4 1.0 convolution_dynamic-update-slice_fusion.4
  21.5 0.6 copy-done.15
  22.3 0.1 copy.130
  22.3 0.1 reshape.163
  22.5 1.5 gather_fusion
  24.0 0.1 reshape.166
  24.3 0.1 copy.133
  24.3 0.1 reshape.168
  24.5 1.5 gather_fusion.1
  26.0 0.1 reshape.171
  26.4 0.1 reshape.173
  26.5 1.5 gather_fusion.2
  28.1 0.1 reshape.176
  28.3 0.1 copy.138
  28.4 0.2 fusion.31
  28.6 0.3 copy.139
  29.2 0.3 fusion
  29.5 12.0 %psum.14 = f32[2048]{0:T(1024)S(1)} all-reduce(f32[2048]{0:T(1024)S(1)} %fusion), channel_id=1, replica_groups=mesh['kv_0'=4,'kv_1'=4,'tp'=8] {'kv_0'}, use_global_device_ids=true, to_apply=%region_1.0 | all-reduce | flops 2048 | bytes 16384 | tf_op jit(solution)/shard_map/psum | solution.py:17
  41.6 9.5 %psum.15 = f32[2048]{0:T(1024)S(1)} all-reduce(f32[2048]{0:T(1024)S(1)} %psum.14), channel_id=1, replica_groups=mesh['kv_0'=4,'kv_1'=4,'tp'=8] {'kv_1'}, use_global_device_ids=true, to_apply=%region_2.0 | all-reduce | flops 2048 | bytes 16384 | tf_op jit(solution)/shard_map/psum | solution.py:17
  51.1 80.0 %reduce-scatter.2.cloned.1.call-done = f32[128,1540]{0,1:T(8,128)} async-done(((f32[2048,1540]{0,1:T(8,128)}), f32[128,1540]{0,1:T(8,128)}) %reduce-scatter.2.cloned.1.call-update) | async-done | bytes 788496 | tf_op jit(solution)/shard_map/reduce_scatter | solution.py:24
  131.1 0.7 slice_multiply_fusion.4
  131.9 0.1 reshape.122
  132.0 0.5 fusion.30
  132.5 0.1 add.130
  132.6 0.1 copy.144
  132.7 0.2 fusion.21
  133.0 0.1 copy.145
  133.1 0.1 copy.151
  133.2 0.1 copy.146
  133.3 1.0 slice_multiply_fusion.2
  134.3 0.1 copy.127
  134.5 0.1 copy.126
  134.6 1.1 slice_multiply_fusion.1
  135.8 0.1 copy.125
  135.9 0.2 reshape.119
  136.1 0.1 copy.164
  136.2 0.3 fusion.27
  136.5 0.1 multiply_add_fusion.1
  136.7 0.5 fusion.23
  137.2 0.1 copy.167
  137.3 0.7 fusion.45
  138.0 0.1 copy.156
  138.1 0.1 copy.149
  138.2 0.1 copy.157
  138.3 0.7 convolution_bitcast_fusion.1
  139.0 7.6 %multiply_add_fusion = f32[32,2,128,256]{3,2,1,0:T(8,128)S(1)} fusion(f32[32,2,128,256]{3,2,1,0:T(8,128)} %param.31, f32[32,2]{1,0:T(8,128)S(1)} %copy.150, bf16[32,4,2,256]{3,1,2,0:T(4,128)(2,1)S(1)} %bitcast.79, f32[32,4,2]{1,2,0:T(2,128)S(1)} %copy.151, bf16[32,4,256]{2,1,0:T(4,128)(2,1)S(1)} %copy-done.6), kind=kOutput, calls=%fused_computation.3 | convolution fusion | flops 104923136 | bytes 16975104 | tf_op jit(solution)/shard_map/sph,sphd,sphv->shdv/dot_general | solution.py:81
  146.7 4.6 %multiply_reduce_fusion = (f32[32,4,2]{1,2,0:T(2,128)S(1)}, f32[32,4,2,256]{3,1,2,0:T(4,128)S(1)}) fusion(f32[32,4,2]{1,2,0:T(2,128)S(1)} %copy.157, f32[32,4,2,256]{3,1,2,0:T(4,128)S(1)} %convolution_bitcast_fusion.1, f32[32,2,128,256]{3,2,1,0:T(8,128)S(1)} %multiply_add_fusion, f32[32,4,2,128]{3,2,1,0:T(2,128)S(1)} %reshape.121, f32[32,4,2]{1,2,0:T(2,128)S(1)} %copy.149), kind=kOutput, calls=%fused_computation.30 | convolution fusion | flops 100990720 | bytes 9047040 | tf_op jit(solution)/shard_map/sthd,shdv->sthv/dot_general | solution.py:103
  151.3 0.1 copy.158
  151.4 0.1 copy.159
  151.5 0.1 copy.160
  151.6 0.2 div.41
  151.8 0.1 fusion.15
  152.0 0.1 copy.162
  152.1 0.2 broadcast_in_dim.87
  152.3 31.3 %all_to_all.10 = bf16[16,128,512]{2,1,0:T(8,128)(2,1)S(1)} all-to-all(bf16[16,128,512]{2,1,0:T(8,128)(2,1)S(1)} %broadcast_in_dim.87), channel_id=1, replica_groups=mesh['kv_0'=4,'kv_1'=4,'tp'=8] {'kv_0','kv_1'}, dimensions={0} | all-to-all | bytes 4194304 | tf_op jit(solution)/shard_map/all_to_all | solution.py:30
  183.6 0.7 convolution_convert_fusion
  184.3 21.7 %all_to_all.11 = bf16[8,256,256]{2,1,0:T(8,128)(2,1)S(1)} all-to-all(bf16[8,256,256]{2,1,0:T(8,128)(2,1)S(1)} %bitcast.76), channel_id=1, replica_groups=mesh['kv_0'=4,'kv_1'=4,'tp'=8] {'tp'}, dimensions={0} | all-to-all | bytes 2097152 | tf_op jit(solution)/shard_map/all_to_all | solution.py:52
  206.1 0.8 reduce_sum.42
  (67 shorter events, 1.5 us)
Async XLA Ops:
  7.2 7.8 %copy-start = (bf16[256,512]{1,0:T(8,128)(2,1)S(1)}, bf16[256,512]{1,0:T(8,128)(2,1)}, u32[]{:S(2)}) copy-start(bf16[256,512]{1,0:T(8,128)(2,1)} %param.25) | copy-start | bytes 786436
  7.2 7.8 %copy-start.3 = (bf16[2048,256]{1,0:T(8,128)(2,1)S(1)}, bf16[2048,256]{1,0:T(8,128)(2,1)}, u32[]{:S(2)}) copy-start(bf16[2048,256]{1,0:T(8,128)(2,1)} %param.21) | copy-start | bytes 3145732
  7.2 123.9 %reduce-scatter.2.cloned.1.call-start = ((), (), s32[]{:S(2)}) async-start(), calls=%async_computation.3 | async-start | bytes 13438976 | tf_op jit(solution)/shard_map/reduce_scatter | solution.py:24
  11.9 5.8 %copy-start.4 = (bf16[256,512]{1,0:T(8,128)(2,1)S(1)}, bf16[256,512]{1,0:T(8,128)(2,1)}, u32[]{:S(2)}) copy-start(bf16[256,512]{1,0:T(8,128)(2,1)} %param.26) | copy-start | bytes 786436
  21.4 0.7 copy-start.15
  21.4 1.0 copy-start.1
  26.5 2.5 %copy-start.16 = (s32[32]{0:T(128)S(1)}, s32[32]{0:T(128)}, u32[]{:S(2)}) copy-start(s32[32]{0:T(128)} %param.38) | copy-start | bytes 388
  26.5 2.5 %copy-start.11 = (f32[32,4,2]{0,2,1:T(2,128)S(1)}, f32[32,4,2]{0,2,1:T(2,128)}, u32[]{:S(2)}) copy-start(f32[32,4,2]{0,2,1:T(2,128)} %param.37) | copy-start | bytes 3076
  26.5 2.5 %copy-start.9 = (f32[32,4,2]{0,2,1:T(2,128)S(1)}, f32[32,4,2]{0,2,1:T(2,128)}, u32[]{:S(2)}) copy-start(f32[32,4,2]{0,2,1:T(2,128)} %param.36) | copy-start | bytes 3076
  26.5 2.5 %copy-start.13 = (f32[32,2]{0,1:T(2,128)S(1)}, f32[32,2]{0,1:T(2,128)}, u32[]{:S(2)}) copy-start(f32[32,2]{0,1:T(2,128)} %param.33) | copy-start | bytes 772
  26.5 2.6 %copy-start.12 = (f32[512]{0:T(512)S(1)}, f32[512]{0:T(512)}, u32[]{:S(2)}) copy-start(f32[512]{0:T(512)} %param.29) | copy-start | bytes 6148
  28.0 108.1 %copy-start.6 = (bf16[32,4,256]{2,1,0:T(4,128)(2,1)S(1)}, bf16[32,4,256]{2,1,0:T(4,128)(2,1)}, u32[]{:S(2)}) copy-start(bf16[32,4,256]{2,1,0:T(4,128)(2,1)} %param.34) | copy-start | bytes 196612
  28.1 108.5 %copy-start.7 = (f32[32,2,128]{2,1,0:T(2,128)S(1)}, f32[32,2,128]{2,1,0:T(2,128)}, u32[]{:S(2)}) copy-start(f32[32,2,128]{2,1,0:T(2,128)} %param.32) | copy-start | bytes 98308
  29.1 109.0 %copy-start.10 = (f32[32,2]{0,1:T(2,128)}, f32[32,2]{0,1:T(2,128)S(1)}, u32[]{:S(2)}) copy-start(f32[32,2]{0,1:T(2,128)S(1)} %get-tuple-element.8) | copy-start | bytes 772
  134.4 4.7 %copy-start.5 = (bf16[32,4,512]{2,1,0:T(4,128)(2,1)S(1)}, bf16[32,4,512]{2,1,0:T(4,128)(2,1)}, u32[]{:S(2)}) copy-start(bf16[32,4,512]{2,1,0:T(4,128)(2,1)} %param.35) | copy-start | bytes 393220
  136.6 10.0 %copy-start.8 = (f32[32,2,128]{2,1,0:T(2,128)}, f32[32,2,128]{2,1,0:T(2,128)S(1)}, u32[]{:S(2)}) copy-start(f32[32,2,128]{2,1,0:T(2,128)S(1)} %multiply_add_fusion.1) | copy-start | bytes 98308
  146.7 4.6 %copy-start.2 = (f32[32,2,128,256]{3,2,1,0:T(8,128)}, f32[32,2,128,256]{3,2,1,0:T(8,128)S(1)}, u32[]{:S(2)}) copy-start(f32[32,2,128,256]{3,2,1,0:T(8,128)S(1)} %multiply_add_fusion) | copy-start | bytes 25165828
  151.6 32.0 %copy-start.14 = (bf16[512,256]{1,0:T(8,128)(2,1)S(1)}, bf16[512,256]{1,0:T(8,128)(2,1)}, u32[]{:S(2)}) copy-start(bf16[512,256]{1,0:T(8,128)(2,1)} %param.30) | copy-start | bytes 786436
Sparse Core Ops, SparseCore 0:
  21.6 109.4 reduce-scatter.1
where the time goes:
time: 214 us
  waiting for transfers between devices  80 us (37%)
  blocking collectives  74.5 us (35%)
  matrix products  28.3 us (13%)
  between operations  14.5 us (7%)
  local copies, waits for them, and re-layouts  11.2 us (5%)
  other arithmetic  5.09 us (2%)
    reduce_scatter x1, waiting for transfers between devices, sent_together(): filled = lax.psum_scatter(both, axis, scatter_dimension=dim, tiled=True)  80 us
    all_to_all x1, blocking collectives, from_everyone(): return lax.all_to_all(copies, axis, split_axis=0, concat_axis=0, tiled=True)  31.3 us
    all_to_all x1, blocking collectives, sum_at_owner(): lax.all_to_all(blocks, axis, split_axis=0, concat_axis=0, tiled=True)  21.7 us
    psum x2, blocking collectives, over_axes(): value = lax.psum(value, axis)  21.5 us
    dot_general x1, matrix products, commit(): jnp.einsum('sph,sphd,sphv->shdv', weights, prior_k, prior_v, precision=hp)  7.63 us
    gather x15, local copies, waits for them, and re-layouts, ancestry(): looked = jnp.take_along_axis(parents, jnp.maximum(current, 0), axis=1)  5.63 us
    dot_general x1, matrix products, tree_read(): jnp.einsum('sthd,shdv->sthv', query, matrix, precision=hp)  4.58 us
  transfers between devices with their start and end apart: 1, of which 1 were waited for; matrix products, arithmetic and copies ran while one was open for 3% of the time, Pallas kernels for 0%

commit v1 on v0

v1 whole, which is shorter than its diff:
```python
import functools

import jax
import jax.numpy as jnp
from jax import lax
from jax.experimental import pallas as pl
from jax.experimental.pallas import tpu as pltpu
from jax.sharding import Mesh
from jax.sharding import PartitionSpec as P

D = 4096
HEADS = 16
DQK = 128
DV = 256
PROP = 4
KV = ("z", "y")
TP = ("x", "c")
RING = 4
BLOCK = 128
WIDE = 256
UNITS = 6
MESH = pl.DeviceIdType.MESH
f32 = jnp.float32
bf16 = jnp.bfloat16
NEG = -1e30


def ring_of(axis):
    me = lax.axis_index(axis)
    return me, lax.rem(me + 1, RING), lax.rem(me + RING - 1, RING), lax.rem(me + 2, RING)


def iota(shape, dim):
    return lax.broadcasted_iota(jnp.int32, shape, dim)


def meet(peers):
    barrier = pltpu.get_barrier_semaphore()
    for peer in peers:
        pl.semaphore_signal(barrier, inc=1, device_id=peer, device_id_type=MESH)
    pl.semaphore_wait(barrier, len(peers))


def send(src, dst, ssem, rsem, peer):
    copy = pltpu.make_async_remote_copy(
        src_ref=src, dst_ref=dst, send_sem=ssem, recv_sem=rsem, device_id=peer, device_id_type=MESH
    )
    copy.start()
    return copy


def project_kernel(
    x_ref, gain_ref, wq_ref, wk_ref, wv_ref, wo_ref, wg_ref, y_ref, g_ref,
    normed, m1, m2, dep, m3, own, r1, r2, r3, n1, n2, n3, q1, q2, q3,
    gall, gin, gsum, gin2, ssem, rsem, gssem, grsem,
):
    rings = {"z": ring_of("z"), "y": ring_of("y")}
    meet([{a: rings[a][k]} for a in ("z", "y") for k in (1, 2, 3)])
    me_kv = rings["z"][0] * RING + rings["y"][0]
    gain = gain_ref[pl.ds(2 * me_kv, 2), :]
    gain = jnp.concatenate([gain[0:1], gain[1:2]], axis=1)

    def norm_block(k, carry):
        normed[k] = (x_ref[pl.ds(pl.multiple_of(k * BLOCK, BLOCK), BLOCK), :].astype(f32) * gain).astype(bf16)
        return carry

    lax.fori_loop(0, RING * RING, norm_block, 0)

    def rows_of(axis, group):
        if axis == "z":
            part = normed[pl.ds(group * RING, RING)]
        else:
            part = jnp.concatenate([normed[pl.ds(k * RING + group, 1)] for k in range(RING)], axis=0)
        return part.reshape(RING * BLOCK, WIDE)

    def weight(unit):
        lane, c = divmod(unit, 3)
        if lane == 0:
            return (wq_ref[...], wk_ref[...], wo_ref[:, :WIDE])[c]
        return (wv_ref[:, :WIDE], wv_ref[:, WIDE:], wo_ref[:, WIDE:])[c]

    def out_cols(unit):
        lane, c = divmod(unit, 3)
        at = ((0, 256, 1024) if lane == 0 else (512, 768, 1280))[c]
        return slice(at, at + WIDE)

    axes_of = lambda unit: ("z", "y") if unit < 3 else ("y", "z")
    sent = []
    arrived = {}
    half = RING * BLOCK // 2

    def ship(stage, unit, kind, way, src, dst):
        axis = axes_of(unit)[stage]
        slot = ((stage * UNITS + unit) * 3 + kind) * 2 + way
        copy = send(src, dst, ssem.at[slot], rsem.at[slot], {axis: rings[axis][1 + way]})
        sent.append(copy)
        arrived[(stage, unit, kind, way)] = copy

    order = [0, 3, 1, 4, 2, 5]
    for unit in order:
        axis = axes_of(unit)[0]
        me, nxt, prv, opp = rings[axis]
        w = weight(unit)
        part = jnp.dot(rows_of(axis, opp), w, preferred_element_type=f32).astype(bf16)
        m1[unit, 0] = part[:half]
        m1[unit, 1] = part[half:]
        ship(0, unit, 0, 0, m1.at[unit, 0], r1.at[unit, 0])
        ship(0, unit, 0, 1, m1.at[unit, 1], r1.at[unit, 1])
        part = jnp.dot(rows_of(axis, nxt), w, preferred_element_type=f32)
        dep[unit, 0] = part[:half]
        m2[unit, 0] = part[half:].astype(bf16)
        ship(0, unit, 1, 0, m2.at[unit, 0], r2.at[unit, 0])
        part = jnp.dot(rows_of(axis, prv), w, preferred_element_type=f32)
        dep[unit, 1] = part[half:]
        m2[unit, 1] = part[:half].astype(bf16)
        ship(0, unit, 1, 1, m2.at[unit, 1], r2.at[unit, 1])
        own[unit] = jnp.dot(rows_of(axis, me), w, preferred_element_type=f32).reshape(RING, BLOCK, WIDE)

    tp_at = lax.axis_index("x") * 2 + lax.axis_index("c")
    row = iota((8, 32), 0)
    col = iota((8, 32), 1)
    pick = jnp.where(row < 2, 2 * tp_at + row, jnp.where(row < 4, HEADS + 2 * tp_at + row - 2, -1))
    wg = jnp.dot((pick == col).astype(bf16), wg_ref[...], preferred_element_type=f32).astype(bf16)
    ones = (iota((8, WIDE), 0) == 4).astype(bf16)
    lanes = (((1,), (1,)), ((), ()))
    for group in range(RING):
        xs = x_ref[group * 512 : (group + 1) * 512, :].astype(f32)
        squares = xs * xs
        high = squares.astype(bf16)
        low = (squares - high.astype(f32)).astype(bf16)
        tile = lax.dot_general(wg, normed[group * RING : (group + 1) * RING].reshape(512, WIDE), lanes, preferred_element_type=f32)
        tile += lax.dot_general(ones, high, lanes, preferred_element_type=f32)
        tile += lax.dot_general(ones, low, lanes, preferred_element_type=f32)
        gall[group] = tile
    gates1 = []
    for k in (1, 2, 3):
        peer = rings["z"][k]
        gates1.append(send(gall.at[peer], gin.at[k - 1], gssem.at[k - 1], grsem.at[k - 1], {"z": peer}))

    def finish_first(unit):
        axis = axes_of(unit)[0]
        for way in range(2):
            arrived[(0, unit, 0, way)].wait_recv()
            m3[unit, way] = (dep[unit, way] + r1[unit, way].astype(f32)).astype(bf16)
            ship(0, unit, 2, way, m3.at[unit, way], r3.at[unit, way])

    for unit in order:
        finish_first(unit)

    for copy in gates1:
        copy.wait_recv()
    total = gall[rings["z"][0]] + gin[0] + gin[1] + gin[2]
    for k in range(RING):
        gsum[k] = total[:, k * BLOCK : (k + 1) * BLOCK]
    gates2 = []
    for k in (1, 2, 3):
        peer = rings["y"][k]
        gates2.append(send(gsum.at[peer], gin2.at[k - 1], gssem.at[k + 2], grsem.at[k + 2], {"y": peer}))

    quarter = BLOCK // 2
    for unit in order:
        axis = axes_of(unit)[1]
        me, nxt, prv, opp = rings[axis]
        for way in range(2):
            arrived[(0, unit, 1, way)].wait_recv()
            arrived[(0, unit, 2, way)].wait_recv()
        low = own[unit, 0:2].reshape(half, WIDE) + r3[unit, 0].astype(f32) + r2[unit, 1].astype(f32)
        high = own[unit, 2:4].reshape(half, WIDE) + r2[unit, 0].astype(f32) + r3[unit, 1].astype(f32)
        own[unit, 0:2] = low.reshape(2, BLOCK, WIDE)
        own[unit, 2:4] = high.reshape(2, BLOCK, WIDE)
        n1[unit, 0] = own[unit, opp, :quarter].astype(bf16)
        n1[unit, 1] = own[unit, opp, quarter:].astype(bf16)
        ship(1, unit, 0, 0, n1.at[unit, 0], q1.at[unit, 0])
        ship(1, unit, 0, 1, n1.at[unit, 1], q1.at[unit, 1])
        n2[unit, 0] = own[unit, nxt, quarter:].astype(bf16)
        ship(1, unit, 1, 0, n2.at[unit, 0], q2.at[unit, 0])
        n2[unit, 1] = own[unit, prv, :quarter].astype(bf16)
        ship(1, unit, 1, 1, n2.at[unit, 1], q2.at[unit, 1])

    for unit in order:
        axis = axes_of(unit)[1]
        me, nxt, prv, opp = rings[axis]
        arrived[(1, unit, 0, 0)].wait_recv()
        n3[unit, 0] = (own[unit, nxt, :quarter] + q1[unit, 0].astype(f32)).astype(bf16)
        ship(1, unit, 2, 0, n3.at[unit, 0], q3.at[unit, 0])
        arrived[(1, unit, 0, 1)].wait_recv()
        n3[unit, 1] = (own[unit, prv, quarter:] + q1[unit, 1].astype(f32)).astype(bf16)
        ship(1, unit, 2, 1, n3.at[unit, 1], q3.at[unit, 1])

    for copy in gates2:
        copy.wait_recv()
    g_ref[...] = gsum[rings["y"][0]] + gin2[0] + gin2[1] + gin2[2]

    for unit in order:
        me = rings[axes_of(unit)[1]][0]
        for way in range(2):
            arrived[(1, unit, 1, way)].wait_recv()
            arrived[(1, unit, 2, way)].wait_recv()
        cols = out_cols(unit)
        y_ref[:quarter, cols] = own[unit, me, :quarter] + q3[unit, 0].astype(f32) + q2[unit, 1].astype(f32)
        y_ref[quarter:, cols] = own[unit, me, quarter:] + q2[unit, 0].astype(f32) + q3[unit, 1].astype(f32)

    for copy in sent + gates1 + gates2:
        copy.wait_send()


def project(tokens, norm_gain, query_weight, key_weight, value_weight, outgate_weight, gate_weight):
    vmem = pl.BlockSpec(memory_space=pltpu.VMEM)
    first = lambda kind: pltpu.VMEM((UNITS, 2, 256, WIDE), kind)
    second = pltpu.VMEM((UNITS, 2, 64, WIDE), bf16)
    return pl.pallas_call(
        project_kernel,
        out_shape=(jax.ShapeDtypeStruct((BLOCK, 1536), f32), jax.ShapeDtypeStruct((8, BLOCK), f32)),
        in_specs=[vmem] * 7,
        out_specs=(vmem, vmem),
        scratch_shapes=[
            pltpu.VMEM((16, BLOCK, WIDE), bf16),
            first(bf16), first(bf16), first(f32), first(bf16),
            pltpu.VMEM((UNITS, RING, BLOCK, WIDE), f32),
            first(bf16), first(bf16), first(bf16),
            second, second, second, second, second, second,
            pltpu.VMEM((RING, 8, 512), f32),
            pltpu.VMEM((3, 8, 512), f32),
            pltpu.VMEM((RING, 8, BLOCK), f32),
            pltpu.VMEM((3, 8, BLOCK), f32),
            pltpu.SemaphoreType.DMA((72,)),
            pltpu.SemaphoreType.DMA((72,)),
            pltpu.SemaphoreType.DMA((6,)),
            pltpu.SemaphoreType.DMA((6,)),
        ],
        compiler_params=pltpu.CompilerParams(
            collective_id=0, has_side_effects=True, vmem_limit_bytes=50 * 1024 * 1024
        ),
        cost_estimate=pl.CostEstimate(flops=2 * 2048 * 256 * 1540, bytes_accessed=3_000_000, transcendentals=0),
        name="project",
    )(tokens, norm_gain.reshape(32, 128), query_weight, key_weight, value_weight, outgate_weight, gate_weight.T)


def to_col(row, eye):
    return jnp.sum(jnp.where(eye, row, 0.0), axis=1, keepdims=True)


def to_row(col, eye):
    return jnp.sum(jnp.where(eye, col, 0.0), axis=0, keepdims=True)


SEQ_STEP = 4


def cell_kernel(
    bias_ref, y_ref, g_ref, pk_ref, pv_ref, pi_ref, pf_ref, acc_ref, par_ref, stable_ref, gain_ref, normal_ref, state_ref,
    hidden_ref, state_out, normal_out, stable_out,
    kt, wv, decay, qs, mem, nsrow,
):
    step = pl.program_id(0)
    heads = 2
    eye = iota((BLOCK, BLOCK), 0) == iota((BLOCK, BLOCK), 1)
    seq_of = iota((BLOCK, 32), 0) // PROP == iota((BLOCK, 32), 1)
    place = iota((BLOCK, 32), 0) % PROP

    def spread(rows):
        picked = jnp.broadcast_to(rows[0], (BLOCK, 32))
        for p in range(1, PROP):
            picked = jnp.where(place == p, rows[p], picked)
        return jnp.sum(jnp.where(seq_of, picked, 0.0), axis=1, keepdims=True)

    @pl.when(step == 0)
    def _():
        acc = acc_ref[...].astype(f32)
        live = [acc > p for p in range(PROP)]
        forget = [jnp.where(live[p], pf_ref[p], 0.0) for p in range(PROP)]
        cum = [forget[0]]
        for p in range(1, PROP):
            cum.append(cum[-1] + forget[p])
        total = cum[-1]
        logs = [jnp.where(live[p], total - cum[p] + pi_ref[p], NEG) for p in range(PROP)]
        carried = total + stable_ref[...]
        new_stable = carried
        for p in range(PROP):
            new_stable = jnp.maximum(new_stable, logs[p])
        stable_out[...] = new_stable
        weights = [jnp.where(live[p], jnp.exp(logs[p] - new_stable), 0.0) for p in range(PROP)]
        fade = jnp.exp(carried - new_stable)
        scale_col = to_col(lax.rsqrt(g_ref[4:5] / D + 1e-6), eye)
        seq_pick = iota((32, BLOCK), 0) == iota((32, BLOCK), 1) // PROP
        eye32 = iota((32, 32), 0) == iota((32, 32), 1)
        for h in range(heads):
            wcol = spread([weights[p][h : h + 1] for p in range(PROP)])
            keys = pk_ref[:, h * DQK : (h + 1) * DQK].astype(f32)
            kt[h] = keys.T.astype(bf16)
            wv[h] = (wcol * pv_ref[:, h * DV : (h + 1) * DV].astype(f32)).astype(bf16)
            fcol = jnp.sum(jnp.where(eye32, fade[h : h + 1], 0.0), axis=1, keepdims=True)
            decay[h] = jnp.broadcast_to(fcol, (32, DQK))
            summed = jnp.dot(seq_pick.astype(f32), wcol * keys, preferred_element_type=f32, precision=lax.Precision.HIGHEST)
            new_normal = fcol * normal_ref[:, h, :] + summed
            normal_out[:, h, :] = new_normal
            qs[h] = y_ref[:, h * DQK : (h + 1) * DQK] * scale_col
            nsrow[h] = jnp.broadcast_to(spread([new_stable[h : h + 1]] * PROP), (BLOCK, DQK))

    even = iota((8, DQK), 0) < PROP
    prior_seq = iota((BLOCK, DV), 0) // PROP
    for h in range(heads):
        for pair in range(SEQ_STEP // 2):
            tiles = []
            for k in range(2):
                j = pair * 2 + k
                s = step * SEQ_STEP + j
                rhs = jnp.where(prior_seq == s, wv[h].astype(f32), 0.0).astype(bf16)
                fresh = jnp.dot(kt[h], rhs, preferred_element_type=f32)
                d = decay[h, pl.ds(s, 1), :]
                d = jnp.concatenate([d, d], axis=1)
                tile = d * state_ref[j, h] + fresh
                state_out[j, h] = tile
                tiles.append(tile.astype(bf16))
            at = pl.multiple_of((step * SEQ_STEP + pair * 2) * PROP, 8)
            q8 = qs[h, pl.ds(at, 8), :]
            lhs = jnp.concatenate([jnp.where(even, q8, 0.0), jnp.where(even, 0.0, q8)], axis=1)
            high = lhs.astype(bf16)
            both = jnp.concatenate([high.astype(f32), lhs - high.astype(f32)], axis=0).astype(bf16)
            got = jnp.dot(both, jnp.concatenate(tiles, axis=0), preferred_element_type=f32)
            mem[h, pl.ds(at, 8), :] = got[:8] + got[8:]

    @pl.when(step == pl.num_programs(0) - 1)
    def _():
        scale_row = lax.rsqrt(g_ref[4:5] / D + 1e-6)
        scale_col = to_col(scale_row, eye)
        parent = spread([par_ref[p : p + 1].astype(f32) for p in range(PROP)])
        base = (iota((BLOCK, 1), 0) // PROP * PROP).astype(f32)
        goal = jnp.where(parent < 0, -1.0, parent + base)
        up = (iota((BLOCK, BLOCK), 1).astype(f32) == goal).astype(f32)
        upb = up.astype(bf16)
        up2 = jnp.dot(upb, upb, preferred_element_type=f32)
        up3 = jnp.dot(up2.astype(bf16), upb, preferred_element_type=f32)
        path = (eye.astype(f32) + up + up2 + up3) > 0.5
        for h in range(heads):
            bias = bias_ref[0, h]
            ingate = scale_row * g_ref[h : h + 1]
            logforget = jax.nn.log_sigmoid(scale_row * g_ref[2 + h : 3 + h] + bias)
            b_col = jnp.sum(jnp.where(path, logforget, 0.0), axis=1, keepdims=True)
            b_row = to_row(b_col, eye)
            dlog = jnp.where(path, b_col - b_row + ingate, NEG)
            ns = nsrow[h]
            carried = b_col + ns[:, 0:1]
            top = jnp.maximum(carried, jnp.max(dlog, axis=1, keepdims=True))
            query = qs[h]
            keys = y_ref[:, 256 + h * DQK : 256 + (h + 1) * DQK] * (scale_col * DQK**-0.5)
            values = y_ref[:, 512 + h * DV : 512 + (h + 1) * DV] * scale_col
            outgate = y_ref[:, 1024 + h * DV : 1024 + (h + 1) * DV] * scale_col
            dots = lax.dot_general(
                query, keys, (((1,), (1,)), ((), ())), preferred_element_type=f32, precision=lax.Precision.HIGHEST
            )
            scores = dots * jnp.where(path, jnp.exp(dlog - top), 0.0)
            factor = jnp.exp(carried - top)
            numer = jnp.dot(scores, values, preferred_element_type=f32, precision=lax.Precision.HIGHEST) + factor * mem[h]
            normal = jnp.dot(
                seq_of.astype(f32), normal_out[:, h, :], preferred_element_type=f32, precision=lax.Precision.HIGHEST
            )
            denom = jnp.sum(scores, axis=1, keepdims=True) + factor * jnp.sum(query * normal, axis=1, keepdims=True)
            read = numer / jnp.maximum(jnp.abs(denom), jnp.exp(-top))
            mean = jnp.sum(read * read, axis=1, keepdims=True) / DV
            gain = gain_ref[:, h * DV : (h + 1) * DV]
            hidden = read * lax.rsqrt(mean + 1e-6) * gain * jax.nn.sigmoid(outgate)
            hidden_ref[:, h * DV : (h + 1) * DV] = hidden.astype(bf16)


def cell(y, g, bias, prior_keys, prior_values, prior_ingate, prior_forget, accepted, parents, stable, gain, normal, state):
    whole = lambda a: pl.BlockSpec(a.shape, lambda i: (0,) * a.ndim)
    small = [
        y, g, prior_keys.reshape(BLOCK, 256), prior_values.reshape(BLOCK, 512),
        prior_ingate.transpose(1, 2, 0), prior_forget.transpose(1, 2, 0),
        accepted.reshape(1, 32), parents.T, stable.T, gain.reshape(1, 512), normal,
    ]
    block = pl.BlockSpec((SEQ_STEP, 2, DQK, DV), lambda i: (i, 0, 0, 0))
    hidden, new_matrix, new_normal, new_stable = pl.pallas_call(
        cell_kernel,
        grid=(32 // SEQ_STEP,),
        out_shape=(
            jax.ShapeDtypeStruct((BLOCK, 512), bf16),
            jax.ShapeDtypeStruct((32, 2, DQK, DV), f32),
            jax.ShapeDtypeStruct((32, 2, DQK), f32),
            jax.ShapeDtypeStruct((2, 32), f32),
        ),
        in_specs=[pl.BlockSpec(memory_space=pltpu.SMEM)] + [whole(a) for a in small] + [block],
        out_specs=(
            pl.BlockSpec((BLOCK, 512), lambda i: (0, 0)),
            block,
            pl.BlockSpec((32, 2, DQK), lambda i: (0, 0, 0)),
            pl.BlockSpec((2, 32), lambda i: (0, 0)),
        ),
        scratch_shapes=[
            pltpu.VMEM((2, DQK, BLOCK), bf16),
            pltpu.VMEM((2, BLOCK, DV), bf16),
            pltpu.VMEM((2, 32, DQK), f32),
            pltpu.VMEM((2, BLOCK, DQK), f32),
            pltpu.VMEM((2, BLOCK, DV), f32),
            pltpu.VMEM((2, BLOCK, DQK), f32),
        ],
        compiler_params=pltpu.CompilerParams(dimension_semantics=("arbitrary",)),
        cost_estimate=pl.CostEstimate(flops=2 * 2048 * 256 * 64, bytes_accessed=17_000_000, transcendentals=0),
        name="cell",
    )(bias, *small, state)
    return hidden, new_matrix, new_normal, new_stable.T


def output_kernel(
    hidden_ref, w_ref, out_ref, gathered, part, mine, got, total, m1, m2, m3, r1, r2, r3, ssem, rsem, psem, qsem, xssem, xrsem
):
    rings = {a: ring_of(a) for a in ("z", "y", "x")}
    core = lax.axis_index("c")
    other = 1 - core
    meet([{a: rings[a][k]} for a in ("z", "y", "x") for k in (1, 2)] + [{"c": other}])
    zme, yme = rings["z"][0], rings["y"][0]
    gathered[zme, yme] = hidden_ref[...]
    sent = []
    arrived = {}
    counter = [0]
    cols = (slice(0, 256), slice(256, 512))

    def ship(key, lane, stage, way, z, y, lo, hi):
        axis = (("z", "y"), ("y", "z"))[lane][stage]
        ref = gathered.at[z, y, lo:hi, cols[lane]]
        slot = counter[0]
        counter[0] += 1
        copy = send(ref, ref, ssem.at[slot], rsem.at[slot], {axis: rings[axis][1 + way]})
        sent.append(copy)
        arrived[key] = copy

    def spot(lane, first, second):
        return (first, second) if lane == 0 else (second, first)

    firsts = (rings["z"], rings["y"])
    seconds = (rings["y"], rings["z"])
    half = BLOCK // 2
    for lane in range(2):
        z, y = spot(lane, firsts[lane][0], seconds[lane][0])
        for way in range(2):
            ship((lane, "a", way), lane, 0, way, z, y, 0, BLOCK)
    for lane in range(2):
        z, y = spot(lane, firsts[lane][0], seconds[lane][0])
        for way in range(2):
            ship((lane, "own", way), lane, 1, way, z, y, 0, BLOCK)
    for lane in range(2):
        me, nxt, prv, opp = firsts[lane]
        second = seconds[lane][0]
        for way, source in ((0, prv), (1, nxt)):
            arrived[(lane, "a", way)].wait_recv()
            z, y = spot(lane, source, second)
            lo, hi = (0, half) if way == 0 else (half, BLOCK)
            ship((lane, "b", way), lane, 0, way, z, y, lo, hi)
            for w in range(2):
                ship((lane, "near", way, w), lane, 1, w, z, y, 0, BLOCK)
    for lane in range(2):
        me, nxt, prv, opp = firsts[lane]
        sme, snxt, sprv, sopp = seconds[lane]
        for way in range(2):
            arrived[(lane, "b", way)].wait_recv()
        z, y = spot(lane, opp, sme)
        for w in range(2):
            ship((lane, "far", w), lane, 1, w, z, y, 0, BLOCK)
        for name, at in (("own", me), (("near", 0), prv), (("near", 1), nxt)):
            for w, source in ((0, sprv), (1, snxt)):
                key = (lane, name, w) if isinstance(name, str) else (lane, *name, w)
                arrived[key].wait_recv()
                z, y = spot(lane, at, source)
                lo, hi = (0, half) if w == 0 else (half, BLOCK)
                ship((lane, "on", name, w), lane, 1, w, z, y, lo, hi)
    for lane in range(2):
        me, nxt, prv, opp = firsts[lane]
        sme, snxt, sprv, sopp = seconds[lane]
        for w, source in ((0, sprv), (1, snxt)):
            arrived[(lane, "far", w)].wait_recv()
            z, y = spot(lane, opp, source)
            lo, hi = (0, half) if w == 0 else (half, BLOCK)
            ship((lane, "on", "far", w), lane, 1, w, z, y, lo, hi)
    for lane in range(2):
        for name in ("own", ("near", 0), ("near", 1), "far"):
            for w in range(2):
                arrived[(lane, "on", name, w)].wait_recv()

    xme, xnxt, xprv, xopp = rings["x"]
    pairs = []
    for group in range(RING):
        z = (xopp, xnxt, xprv, xme)[group]
        rows = gathered[z, pl.ds(2 * other, 2)].reshape(256, 512)
        part[group] = jnp.dot(rows, w_ref[...], preferred_element_type=f32).astype(bf16)
        pairs.append(send(part.at[group], got.at[group], psem.at[group], qsem.at[group], {"c": other}))
    for group in range(RING):
        z = (xopp, xnxt, xprv, xme)[group]
        rows = gathered[z, pl.ds(2 * core, 2)].reshape(256, 512)
        mine[group] = jnp.dot(rows, w_ref[...], preferred_element_type=f32)

    xs = {}

    def ship_x(kind, way, src, dst):
        slot = kind * 2 + way
        xs[(kind, way)] = send(src, dst, xssem.at[slot], xrsem.at[slot], {"x": rings["x"][1 + way]})

    pairs[0].wait_recv()
    total[0] = mine[0] + got[0].astype(f32)
    m1[0] = total[0, :BLOCK].astype(bf16)
    m1[1] = total[0, BLOCK:].astype(bf16)
    ship_x(0, 0, m1.at[0], r1.at[0])
    ship_x(0, 1, m1.at[1], r1.at[1])
    pairs[1].wait_recv()
    total[1] = mine[1] + got[1].astype(f32)
    m2[0] = total[1, BLOCK:].astype(bf16)
    ship_x(1, 0, m2.at[0], r2.at[0])
    pairs[2].wait_recv()
    total[2] = mine[2] + got[2].astype(f32)
    m2[1] = total[2, :BLOCK].astype(bf16)
    ship_x(1, 1, m2.at[1], r2.at[1])
    pairs[3].wait_recv()
    total[3] = mine[3] + got[3].astype(f32)
    xs[(0, 0)].wait_recv()
    m3[0] = (total[1, :BLOCK] + r1[0].astype(f32)).astype(bf16)
    ship_x(2, 0, m3.at[0], r3.at[0])
    xs[(0, 1)].wait_recv()
    m3[1] = (total[2, BLOCK:] + r1[1].astype(f32)).astype(bf16)
    ship_x(2, 1, m3.at[1], r3.at[1])
    for kind in (1, 2):
        for way in range(2):
            xs[(kind, way)].wait_recv()
    out_ref[:BLOCK] = (total[3, :BLOCK] + r3[0].astype(f32) + r2[1].astype(f32)).astype(bf16)
    out_ref[BLOCK:] = (total[3, BLOCK:] + r2[0].astype(f32) + r3[1].astype(f32)).astype(bf16)
    for copy in sent + pairs + list(xs.values()):
        copy.wait_send()


def output(hidden, weight):
    vmem = pl.BlockSpec(memory_space=pltpu.VMEM)
    pair = pltpu.VMEM((2, BLOCK, 256), bf16)
    return pl.pallas_call(
        output_kernel,
        out_shape=jax.ShapeDtypeStruct((256, 256), bf16),
        in_specs=[vmem, vmem],
        out_specs=vmem,
        scratch_shapes=[
            pltpu.VMEM((RING, RING, BLOCK, 512), bf16),
            pltpu.VMEM((RING, 256, 256), bf16),
            pltpu.VMEM((RING, 256, 256), f32),
            pltpu.VMEM((RING, 256, 256), bf16),
            pltpu.VMEM((RING, 256, 256), f32),
            pair, pair, pair, pair, pair, pair,
            pltpu.SemaphoreType.DMA((40,)),
            pltpu.SemaphoreType.DMA((40,)),
            pltpu.SemaphoreType.DMA((4,)),
            pltpu.SemaphoreType.DMA((4,)),
            pltpu.SemaphoreType.DMA((6,)),
            pltpu.SemaphoreType.DMA((6,)),
        ],
        compiler_params=pltpu.CompilerParams(
            collective_id=1, has_side_effects=True, vmem_limit_bytes=40 * 1024 * 1024
        ),
        cost_estimate=pl.CostEstimate(flops=2 * 2048 * 256 * 512, bytes_accessed=3_000_000, transcendentals=0),
        name="output",
    )(hidden, weight)


def per_device(
    tokens, norm_gain, query_weight, key_weight, value_weight, outgate_weight, gate_weight, forget_bias, head_gain,
    output_weight, state_matrix, state_normal, state_stable, prior_keys, prior_values, prior_ingate, prior_forget,
    accepted, parents,
):
    y, g = project(tokens, norm_gain, query_weight, key_weight, value_weight, outgate_weight, gate_weight)
    bias = lax.dynamic_slice_in_dim(forget_bias, lax.axis_index(TP) * 2, 2, 0).reshape(1, 2)
    hidden, new_matrix, new_normal, new_stable = cell(
        y, g, bias, prior_keys, prior_values, prior_ingate, prior_forget, accepted, parents, state_stable, head_gain,
        state_normal, state_matrix,
    )
    layer_out = output(hidden, output_weight)
    return layer_out, new_matrix, new_normal, new_stable


def solution(mesh):
    torus = Mesh(mesh.devices.reshape(4, 4, 4, 2), ("z", "y", "x", "c"))
    placed = (
        P(None, KV), P(), P(KV, TP), P(KV, TP), P(KV, TP), P(KV, TP), P(KV, None), P(), P(TP), P(TP, KV),
        P(KV, TP, None, None), P(KV, TP, None), P(KV, TP), P(KV, None, TP), P(KV, None, TP), P(KV, None, TP),
        P(KV, None, TP), P(KV), P(KV, None),
    )
    return jax.shard_map(
        per_device,
        mesh=torus,
        in_specs=placed,
        out_specs=(P(TP, KV), P(KV, TP, None, None), P(KV, TP, None), P(KV, TP)),
        check_vma=False,
    )
```

time: 214 us -> 103 us (0.48)
  Pallas kernels: 0 us -> 86.6 us
  waiting for transfers between devices: 80 us -> 0 us
  blocking collectives: 74.5 us -> 0 us
  matrix products: 28.3 us -> 0 us
  between operations: 14.5 us -> 0.7 us
  other arithmetic: 5.09 us -> 0 us
  local copies, waits for them, and re-layouts: 11.2 us -> 13.7 us
    pallas_call x0 -> x3, Pallas kernels: none -> 86.6 us  [the longest x1 42.1 us: project(): pl.pallas_call(project_kernel, out_shape=(jax.ShapeDtypeStruct((BLOCK, 15...]
    reduce_scatter x1 -> x0, waiting for transfers between devices: 80 us -> none  [sent_together(): filled = lax.psum_scatter(both, axis, scatter_dimension=dim, tiled=True)]
    all_to_all x2 -> x0, blocking collectives: 53 us -> none  [the longest x1 31.3 us: from_everyone(): return lax.all_to_all(copies, axis, split_axis=0, concat_axis=0, tiled=True)]
    dot_general x13 -> x0, matrix products: 28.3 us -> none  [the longest x1 7.63 us: commit(): jnp.einsum('sph,sphd,sphv->shdv', weights, prior_k, prior_v, precision=hp)]
    psum x2 -> x0, blocking collectives: 21.5 us -> none  [over_axes(): value = lax.psum(value, axis)]
    unnamed x35 -> x25, local copies, waits for them, and re-layouts: 0.75 us -> 10 us
    gather x15 -> x0, local copies, waits for them, and re-layouts: 5.63 us -> none  [ancestry(): looked = jnp.take_along_axis(parents, jnp.maximum(current, 0), axis=1)]
    reshape x5 -> x3, local copies, waits for them, and re-layouts: 0.43 us -> 3.68 us  [the longest x1 1.59 us: cell(): prior_values.reshape(BLOCK, 512)]
  transfers between devices with their start and end apart: 1 -> 0, of which waited for: 1 -> 0; matrix products, arithmetic and copies ran while one was open for 3% -> 0% of each run, Pallas kernels for 0% -> 0%
where the time goes in v1:
time: 103 us; the launch traced here: 101 us
  Pallas kernels  86.6 us (84%)
  local copies, waits for them, and re-layouts  13.7 us (13%)
    pallas_call x1, Pallas kernels, project(): pl.pallas_call(project_kernel, out_shape=(jax.ShapeDtypeStruct((BLOCK, 15...  42.1 us
    pallas_call x1, Pallas kernels, output(): pl.pallas_call(output_kernel, out_shape=jax.ShapeDtypeStruct((256, 256),...  30.5 us
    pallas_call x1, Pallas kernels, cell(): pl.pallas_call(cell_kernel, grid=(32 // SEQ_STEP,), out_shape=(jax.ShapeD...  13.9 us
    unnamed x25, local copies, waits for them, and re-layouts  10 us

profile of v1, /device:TPU:1, one launch (start us, length us, event | category | flops | bytes accessed | tf_op | source)
XLA Modules:
  0.0 101.0 jit_solution(4847467552152930334)
XLA Ops:
  0.6 0.0 copy-start
  0.6 0.0 copy-start.6
  0.7 0.6 copy-done
  1.3 0.6 dynamic-slice_bitcast_fusion.bias_ref
  1.9 1.5 %reshape.28.pk_ref = bf16[128,256]{1,0:T(8,128)(2,1)} reshape(bf16[32,4,256]{2,1,0:T(4,128)(2,1)} %param.32) | data formatting | bytes 131072 | tf_op jit(solution)/shard_map/reshape | solution.py:369
  3.4 1.6 %reshape.29.pv_ref = bf16[128,512]{1,0:T(8,128)(2,1)} reshape(bf16[32,4,512]{2,1,0:T(4,128)(2,1)} %param.33) | data formatting | bytes 262144 | tf_op jit(solution)/shard_map/reshape | solution.py:369
  5.0 0.0 copy-start.3
  5.0 1.2 %copy-done.3 = bf16[2048,256]{1,0:T(8,128)(2,1)S(1)} copy-done((bf16[2048,256]{1,0:T(8,128)(2,1)S(1)}, bf16[2048,256]{1,0:T(8,128)(2,1)}, u32[]{:S(2)}) %copy-start.3) | copy-done | bytes 1048600
  6.2 0.0 copy-start.4
  6.2 0.9 copy-done.4
  7.2 0.0 copy-start.5
  7.2 0.9 copy-done.5
  8.1 0.0 copy-start.7
  8.1 0.9 copy-done.7
  9.0 0.0 copy-start.8
  9.0 0.9 copy-done.8
  9.9 0.0 copy-start.10
  9.9 0.7 copy-done.10
  10.6 0.0 copy-start.11
  10.6 0.7 copy-done.11
  11.3 42.1 %project.1 = (f32[128,1536]{1,0:T(8,128)S(1)}, f32[8,128]{1,0:T(8,128)S(1)}) custom-call(bf16[2048,256]{1,0:T(8,128)(2,1)S(1)} %copy-done.3, f32[32,128]{1,0:T(8,128)S(1)} %bitcast.11, bf16[256,256]{1,0:T(8,128)(2,1)S(1)} %copy-done.7, bf16[256,256]{1,0:T(8,128)(2,1)S(1)} %copy-done.8, bf16[256,512]{1,0:T(8,128)(2,1)S(1)} %copy-done.4, ...), custom_call_target="tpu_custom_call" | custom-call | flops 1614807040 | bytes 3000000 | tf_op jit(solution)/shard_map/project/pallas_call | solution.py:211
  53.5 0.0 copy-start.1
  53.5 0.9 copy-done.1
  54.4 0.0 copy-start.2
  54.4 0.6 copy-done.2
  55.0 13.9 %cell.1 = (bf16[128,512]{1,0:T(8,128)(2,1)}, f32[32,2,128,256]{3,2,1,0:T(8,128)}, f32[32,2,128]{2,1,0:T(2,128)}, f32[2,32]{1,0:T(2,128)}) custom-call(f32[1,2]{1,0:T(1,128)} %dynamic-slice_bitcast_fusion.bias_ref, f32[128,1536]{1,0:T(8,128)} %copy-done.1, f32[8,128]{1,0:T(8,128)} %copy-done.2, bf16[128,256]{1,0:T(8,128)(2,1)} %reshape.28.pk_ref, ...), custom_call_target="tpu_custom_call" | custom-call | flops 67108864 | bytes 17000000 | tf_op jit(solution)/shard_map/cell/pallas_call | solution.py:374
  68.9 0.0 copy-done.6
  68.9 0.0 copy-start.9
  68.9 0.9 copy-done.9
  69.8 30.5 %output.1 = bf16[256,256]{1,0:T(8,128)(2,1)S(1)} custom-call(bf16[128,512]{1,0:T(8,128)(2,1)S(1)} %copy-done.9, bf16[512,256]{1,0:T(8,128)(2,1)S(1)} %copy-done.6), custom_call_target="tpu_custom_call" | custom-call | flops 536870912 | bytes 3000000 | tf_op jit(solution)/shard_map/output/pallas_call | solution.py:532
  100.3 0.7 copy.24
Async XLA Ops:
  0.6 0.7 copy-start
  0.6 68.2 %copy-start.6 = (bf16[512,256]{1,0:T(8,128)(2,1)S(1)}, bf16[512,256]{1,0:T(8,128)(2,1)}, u32[]{:S(2)}) copy-start(bf16[512,256]{1,0:T(8,128)(2,1)} %w_ref.1) | copy-start | bytes 786436
  5.0 1.2 %copy-start.3 = (bf16[2048,256]{1,0:T(8,128)(2,1)S(1)}, bf16[2048,256]{1,0:T(8,128)(2,1)}, u32[]{:S(2)}) copy-start(bf16[2048,256]{1,0:T(8,128)(2,1)} %x_ref.1) | copy-start | bytes 3145732
  6.2 0.9 copy-start.4
  7.2 0.9 copy-start.5
  8.1 0.9 copy-start.7
  9.0 0.9 copy-start.8
  9.9 0.7 copy-start.10
  10.6 0.7 copy-start.11
  53.5 0.9 copy-start.1
  54.4 0.6 copy-start.2
  68.9 0.9 copy-start.9
